TPU v7x, 512 devices: a whole 4x4x16 slice. The times are simulated.
512 devices in a mesh: sp: 16 (over z), fs: 4 (over y), tp: 8 (over x, core).
Axes of the slice: x: 4, y: 4, z: 16, core: 2. Of those that a mesh axis runs over, the one named last changes fastest.
Arguments:
- tokens: bfloat16 [8192, 2048], P(('fs', 'sp'), 'tp'), parts along dimension 0, may hold values from -6 to 6
- norm_gain: float32 [2048], replicated, may hold values from 0.1 to 1.9
- w_recept: bfloat16 [2048, 1024], P('sp', 'tp'), may hold values from -0.125 to 0.125
- w_key_a: bfloat16 [2048, 1024], P('sp', 'tp'), may hold values from -0.125 to 0.125
- w_value_a: bfloat16 [2048, 1024], P('sp', 'tp'), may hold values from -0.125 to 0.125
- w_gate_a: bfloat16 [2048, 1024], P('sp', 'tp'), may hold values from -0.125 to 0.125
- decay_down_weight: bfloat16 [2048, 64], replicated, may hold values from -0.125 to 0.125
- decay_up_weight: bfloat16 [64, 1024], P(None, 'tp'), may hold values from -0.75 to 0.75
- rate_down_weight: bfloat16 [2048, 64], replicated, may hold values from -0.125 to 0.125
- rate_up_weight: bfloat16 [64, 1024], P(None, 'tp'), may hold values from -0.75 to 0.75
- decay_base: float32 [1024], P('tp'), may hold values from -12 to -2.5
- rate_base: float32 [1024], P('tp'), may hold values from -12 to 1
- rate_shift: float32 [8192, 16], P(('fs', 'sp'), 'tp'), parts along dimension 0, may hold values from 0 to 1.39
- jolts: float32 [8192, 16], P(('fs', 'sp'), 'tp'), parts along dimension 0, may hold values from 0 to 0.69
- group_gain: float32 [1024], P('tp'), may hold values from 0.1 to 1.9
- w_query_b: bfloat16 [2048, 1024], P('sp', 'tp'), may hold values from -0.125 to 0.125
- w_key_b: bfloat16 [2048, 1024], P('sp', 'tp'), may hold values from -0.125 to 0.125
- w_value_b: bfloat16 [2048, 1024], P('sp', 'tp'), may hold values from -0.125 to 0.125
- w_gate_b: bfloat16 [2048, 1024], P('sp', 'tp'), may hold values from -0.125 to 0.125
- score_offset: float32 [8], P('tp'), may hold values from -12 to -1
- w_out_a: bfloat16 [1024, 2048], P('tp'), may hold values from -0.125 to 0.125
- w_out_b: bfloat16 [1024, 2048], P('tp'), may hold values from -0.125 to 0.125
Outputs:
- mixed: bfloat16 [8192, 2048], P(('fs', 'sp', 'tp')), parts along dimension 0
- row_log: float32 [8192, 8], P(('fs', 'sp'), 'tp'), parts along dimension 0
There are 4 independent parts, one for each index of `fs`. A program takes and returns all parts, laid end to end along the dimension named above; an argument that names none is the same for every part. Nothing has to cross between parts.
All inputs are finite; a program needn't handle non-finite values.
Results may differ from a plain program's by a relative error of at most 0.02.
Values may be sent and summed in bfloat16 or wider, within the bound.
No kernel may reach another device: no remote copies, remote signals or barrier semaphores. Data moves between devices by JAX's collectives and lax.ppermute only.
A program may use at most 64 MiB of HBM per device.

v0:
```python
import jax
import jax.numpy as jnp
from jax import lax
from jax.sharding import PartitionSpec as P

HEAD_A = 64
HEAD_B = 128


def copy_for_each(value, axis):
    devices = lax.axis_size(axis)
    return lax.all_to_all(
        jnp.broadcast_to(value[None], (devices, *value.shape)), axis, 0, 0, tiled=True
    )


def laid_out(pieces, dim):
    pieces = jnp.moveaxis(pieces, 0, dim)
    shape = pieces.shape
    return pieces.reshape(*shape[:dim], shape[dim] * shape[dim + 1], *shape[dim + 2 :])


def collect(value, axis, dim):
    pieces = copy_for_each(value, axis)
    return laid_out(pieces, dim)


def in_one_piece(arrays, axis, dim, along):
    ends, at = ([], 0)
    for a in arrays[:-1]:
        at += a.shape[along]
        ends.append(at)
    both = jnp.concatenate(arrays, axis=along)
    return tuple(jnp.split(lax.all_gather(both, axis, axis=dim, tiled=True), ends, axis=along))


def gathered_once(value, axis):
    leaves = jax.tree.leaves(value)
    order = sorted(range(len(leaves)), key=lambda k: -leaves[k].size)
    width = (1, *leaves[order[0]].shape)[-1]
    lines = [
        jnp.pad(leaves[k].reshape(-1), (0, -leaves[k].size % width)).reshape(-1, width)
        for k in order
    ]
    both, at, found = (copy_for_each(jnp.concatenate(lines), axis), 0, {})
    for k, line in zip(order, lines):
        piece = both[:, at : at + len(line)].reshape(len(both), -1)
        found[k] = piece[:, : leaves[k].size].reshape(-1, *leaves[k].shape)
        at += len(line)
    numbers = iter(range(len(leaves)))
    return jax.tree.map(lambda _: found[next(numbers)], value)


def combined_pairwise(pieces, combine):
    while len(jax.tree.leaves(pieces)[0]) > 1:
        pieces = jax.vmap(combine)(
            *(jax.tree.map(lambda part: part[side::2], pieces) for side in (0, 1))
        )
    return jax.tree.map(lambda part: part[0], pieces)


def prefix_2(value, axis, combine, identity):
    devices, index = (lax.axis_size(axis), lax.axis_index(axis))
    passed = jnp.arange(devices) < index

    def kept(part, zero, own):
        part = jnp.where(
            passed.reshape(-1, *(1 for _ in own.shape)),
            part.astype(own.dtype),
            jnp.asarray(zero, own.dtype),
        )
        return part

    pieces = gathered_once(
        jax.tree.map(lambda part, kind: part.astype(kind), value, (jnp.bfloat16, jnp.bfloat16)),
        axis,
    )
    return combined_pairwise(jax.tree.map(kept, pieces, identity, value), combine)


def cut_along(value, dim, devices):
    before, after = (value.shape[:dim], value.shape[dim + 1 :])
    return jnp.moveaxis(value.reshape(*before, devices, -1, *after), dim, 0)


def sent_and_summed(value, axis, dim):
    devices = lax.axis_size(axis)
    pieces = lax.all_to_all(cut_along(value, dim, devices), axis, 0, 0, tiled=True)
    return jnp.sum(pieces.astype(jnp.float32), axis=0)


def combine_states(earlier, follower):
    joined = jnp.einsum("hij,hjk->hik", earlier[0], follower[0])
    carried = jnp.einsum("hij,hjk->hik", earlier[1], follower[0]) + follower[1]
    return (joined, carried)


def block_pass(stacked, pieces):
    recept_c, logs_step, keys_c, values_c, unit_c, mixing_c = pieces
    block_len = recept_c.shape[0]
    totals = jnp.cumsum(logs_step, axis=0)
    preceding = jnp.concatenate([jnp.zeros_like(totals[:1]), totals[:-1]], axis=0)
    steering = unit_c * mixing_c
    places_here = jnp.arange(block_len, dtype=jnp.int32)
    below_diag = (places_here[:, None] > places_here[None, :])[:, :, None, None]
    fading = jnp.where(
        below_diag, jnp.exp(jnp.where(below_diag, preceding[:, None] - totals[None, :], 0.0)), 0.0
    )
    unit_fade = fading * unit_c[:, None]
    weigh_keys = jnp.einsum("tjhc,jhc->htj", unit_fade, keys_c)
    weigh_steer = jnp.einsum("tjhc,jhc->htj", unit_fade, steering)
    read_fade = fading * (recept_c * jnp.exp(logs_step))[:, None]
    diagonal = jnp.eye(block_len, dtype=jnp.float32)
    read_keys = (
        jnp.einsum("tjhc,jhc->htj", read_fade, keys_c)
        + diagonal * jnp.sum(recept_c * keys_c, axis=2).T[:, :, None]
    )
    read_steer = (
        jnp.einsum("tjhc,jhc->htj", read_fade, steering)
        + diagonal * jnp.sum(recept_c * steering, axis=2).T[:, :, None]
    )
    values_wide = jnp.concatenate([jnp.zeros_like(values_c), values_c], axis=2)
    entering = jnp.einsum("thc,hrc->htr", unit_c * jnp.exp(preceding), stacked)
    entering = entering + jnp.einsum("htj,jhr->htr", weigh_keys, values_wide)
    removal = jax.scipy.linalg.solve_triangular(
        weigh_steer + diagonal, entering, lower=True, unit_diagonal=True
    )
    readout = jnp.einsum("thc,hrc->htr", recept_c * jnp.exp(totals), stacked)
    readout = readout + jnp.einsum("htj,jhr->htr", read_keys, values_wide)
    readout = readout - jnp.einsum("htj,hjr->htr", read_steer, removal)
    tail_fade = jnp.exp(totals[-1][None] - totals)
    closing = stacked * jnp.exp(totals[-1])[:, None, :]
    closing = closing + jnp.einsum("jhr,jhc->hrc", values_wide, keys_c * tail_fade)
    closing = closing - jnp.einsum("hjr,jhc->hrc", removal, steering * tail_fade)
    return (closing, jnp.transpose(readout, (1, 0, 2)))


def local(
    tokens,
    norm_gain,
    w_recept,
    w_key_a,
    w_value_a,
    w_gate_a,
    decay_down_weight,
    decay_up_weight,
    rate_down_weight,
    rate_up_weight,
    decay_base,
    rate_base,
    rate_shift,
    jolts,
    group_gain,
    w_query_b,
    w_key_b,
    w_value_b,
    w_gate_b,
    score_offset,
    w_out_a,
    w_out_b,
):
    gathered = collect(tokens, "tp", 1)
    floats = gathered.astype(jnp.float32)
    normed = (
        floats * lax.rsqrt(jnp.mean(floats * floats, axis=1, keepdims=True) + 1e-06) * norm_gain
    ).astype(jnp.bfloat16)
    row_count = normed.shape[0]
    matrices = (w_recept, w_key_a, w_value_a, w_gate_a, w_query_b, w_key_b, w_value_b, w_gate_b)
    portions = in_one_piece(
        (
            matrices[0],
            matrices[1],
            matrices[2],
            matrices[3],
            matrices[4],
            matrices[5],
            matrices[6],
            matrices[7],
        ),
        "sp",
        0,
        1,
    )
    projected = tuple(
        (jnp.dot(normed, portion, preferred_element_type=jnp.float32) for portion in portions)
    )
    recept, keys_a, values_a, gate_a, query_b, keys_b, values_b, gate_b = [
        summed.astype(jnp.bfloat16) for summed in projected
    ]
    heads_a = recept.shape[1] // HEAD_A
    decay_low = jnp.tanh(
        jnp.dot(normed, decay_down_weight, preferred_element_type=jnp.float32)
    ).astype(jnp.bfloat16)
    rate_low = jnp.dot(normed, rate_down_weight, preferred_element_type=jnp.float32).astype(
        jnp.bfloat16
    )
    preact = (
        decay_base
        + jnp.dot(decay_low, decay_up_weight, preferred_element_type=jnp.float32)
        + jnp.repeat(rate_shift, HEAD_A, axis=1)
    )
    log_decay = -jnp.exp(-jax.nn.softplus(-preact) - 0.5) - jnp.repeat(jolts, HEAD_A, axis=1)
    mixing = jax.nn.sigmoid(
        rate_base + jnp.dot(rate_low, rate_up_weight, preferred_element_type=jnp.float32)
    )

    def split_heads(matrix):
        return matrix.astype(jnp.float32).reshape(row_count, heads_a, HEAD_A)

    keys_heads = split_heads(keys_a)
    unit_keys = keys_heads * lax.rsqrt(
        jnp.sum(keys_heads * keys_heads, axis=2, keepdims=True) + 1e-06
    )
    block_len = min(32, row_count)
    block_count = row_count // block_len

    def to_blocks(matrix):
        return matrix.reshape(block_count, block_len, heads_a, HEAD_A)

    inputs = tuple(
        (
            to_blocks(matrix)
            for matrix in (
                split_heads(recept),
                log_decay.reshape(row_count, heads_a, HEAD_A),
                keys_heads,
                split_heads(values_a),
                unit_keys,
                mixing.reshape(row_count, heads_a, HEAD_A),
            )
        )
    )
    identity = jnp.broadcast_to(jnp.eye(HEAD_A, dtype=jnp.float32), (heads_a, HEAD_A, HEAD_A))
    zeros_state = jnp.zeros((heads_a, HEAD_A, HEAD_A), jnp.float32)
    closing, readout = lax.scan(
        block_pass, jnp.concatenate([identity, zeros_state], axis=1), inputs
    )
    readout = readout.reshape(row_count, heads_a, 2 * HEAD_A)
    prefix = prefix_2(
        (closing[:, :HEAD_A], closing[:, HEAD_A:]), "sp", combine_states, (identity, zeros_state)
    )
    outputs_a = readout[:, :, HEAD_A:] + jnp.einsum(
        "hvk,thk->thv", prefix[1], readout[:, :, :HEAD_A]
    )
    centered = outputs_a - jnp.mean(outputs_a, axis=2, keepdims=True)
    normal_a = centered * lax.rsqrt(jnp.mean(centered * centered, axis=2, keepdims=True) + 0.00064)
    mixed_a = (
        normal_a.reshape(row_count, -1) * group_gain * jax.nn.silu(gate_a.astype(jnp.float32))
    ).astype(jnp.bfloat16)
    heads_b = query_b.shape[1] // HEAD_B
    own_index = lax.axis_index("sp")
    places = jnp.arange(row_count, dtype=jnp.int32)
    query_place = own_index * row_count + places
    query_heads = query_b.reshape(row_count, heads_b, HEAD_B)
    factor = HEAD_B ** (-0.5)
    paired = jnp.stack(
        [keys_b.reshape(row_count, heads_b, HEAD_B), values_b.reshape(row_count, heads_b, HEAD_B)]
    )

    def attend(running, paired_piece, source):
        attended, weight_sum, survive = running
        scores = (
            jnp.einsum(
                "qhd,khd->hqk", query_heads, paired_piece[0], preferred_element_type=jnp.float32
            )
            * factor
            + score_offset[:, None, None]
        )
        causal = (source * row_count + places)[None, None, :] < query_place[None, :, None]
        keep_log = jnp.where(causal, jax.nn.log_sigmoid(-scores), 0.0)
        later_sum = (
            jnp.flip(jnp.cumsum(jnp.flip(keep_log, 2), axis=2), 2) - keep_log + survive[:, :, None]
        )
        weights = jnp.where(causal, jnp.exp(jax.nn.log_sigmoid(scores) + later_sum), 0.0)
        attended = attended + jnp.einsum(
            "hqk,khd->qhd",
            weights.astype(jnp.bfloat16),
            paired_piece[1],
            preferred_element_type=jnp.float32,
        )
        return (
            attended,
            weight_sum + jnp.sum(weights, axis=2),
            survive + jnp.sum(keep_log, axis=2),
        )

    empty_b = (
        jnp.zeros((row_count, heads_b, HEAD_B), jnp.float32),
        jnp.zeros((heads_b, row_count), jnp.float32),
        jnp.zeros((heads_b, row_count), jnp.float32),
    )
    running = attend(empty_b, paired, own_index)
    all_pairs = lax.all_gather(paired[None], "sp", axis=0, tiled=True)

    def visit_piece(rounds, holding):
        source = own_index - rounds
        chosen = lax.dynamic_index_in_dim(all_pairs, jnp.maximum(source, 0), 0, False)
        return lax.cond(
            source >= 0, lambda kept: attend(kept, chosen, source), lambda kept: kept, holding
        )

    running = lax.fori_loop(1, lax.axis_size("sp"), visit_piece, running)
    mixed_b = (running[0].reshape(row_count, -1) * jax.nn.silu(gate_b.astype(jnp.float32))).astype(
        jnp.bfloat16
    )
    row_log = jnp.log(jnp.maximum(running[1].T, 0.01))
    mixed = sent_and_summed(
        (
            jnp.dot(mixed_a, w_out_a, preferred_element_type=jnp.float32)
            + jnp.dot(mixed_b, w_out_b, preferred_element_type=jnp.float32)
        ).astype(jnp.bfloat16),
        "tp",
        0,
    )
    return (mixed.astype(jnp.bfloat16), row_log)


def solution(mesh):
    in_specs = (
        P(("fs", "sp"), "tp"),
        P(),
        P("sp", "tp"),
        P("sp", "tp"),
        P("sp", "tp"),
        P("sp", "tp"),
        P(),
        P(None, "tp"),
        P(),
        P(None, "tp"),
        P("tp"),
        P("tp"),
        P(("fs", "sp"), "tp"),
        P(("fs", "sp"), "tp"),
        P("tp"),
        P("sp", "tp"),
        P("sp", "tp"),
        P("sp", "tp"),
        P("sp", "tp"),
        P("tp"),
        P("tp", None),
        P("tp", None),
    )
    out_specs = (P(("fs", "sp", "tp"), None), P(("fs", "sp"), "tp"))
    return jax.shard_map(local, mesh=mesh, in_specs=in_specs, out_specs=out_specs, check_vma=False)
```

profile of v0, /device:TPU:504, one launch (start us, length us, event | category | flops | bytes accessed | tf_op | source)
XLA Modules:
  0.0 244.6 jit_solution(12712214649210133443)
XLA Ops:
  16.1 4.3 %all-to-all-start = ((bf16[8,128,256]{1,2,0:T(8,128)(2,1)}), bf16[8,128,256]{1,2,0:T(8,128)(2,1)S(1)}, u32[]{:S(2)}, u32[]{:S(2)}) async-start(bf16[8,128,256]{1,2,0:T(8,128)(2,1)} %broadcast_in_dim.74), calls=%async_computation | async-start | bytes 1048576 | tf_op jit(solution)/shard_map/all_to_all | solution.py:12
  22.1 8.6 %all-to-all-done = bf16[8,128,256]{1,2,0:T(8,128)(2,1)S(1)} async-done(((bf16[8,128,256]{1,2,0:T(8,128)(2,1)}), bf16[8,128,256]{1,2,0:T(8,128)(2,1)S(1)}, u32[]{:S(2)}, u32[]{:S(2)}) %all-to-all-start) | async-done | bytes 524320 | tf_op jit(solution)/shard_map/all_to_all | solution.py:12
  33.3 56.6 %all-gather.4.cloned.1.call-done = bf16[2048,1024]{1,0:T(8,128)(2,1)} async-done(((bf16[128,1024]{1,0:T(8,128)(2,1)}), bf16[2048,1024]{1,0:T(8,128)(2,1)}) %all-gather.4.cloned.1.call-update) | async-done | bytes 4194320 | tf_op jit(solution)/shard_map/all_gather | solution.py:34
  98.3 48.1 %while.30 = (s32[]{:T(128)}, f32[2,128,64]{1,2,0:T(8,128)S(1)}, f32[4,32,2,128]{3,1,0,2:T(8,128)S(1)}, f32[4,32,2,64]{3,2,1,0:T(2,128)S(1)}, bf16[4,32,2,64]{3,2...) while((s32[]{:T(128)}, f32[2,128,64]{1,2,0:T(8,128)S(1)}, ...), condition=%wide.region_6.7_spmd, body=%wide.region_2.6_spmd.sunk | while | flops 11161506 | bytes 3108997 | solution.py:235
  102.6 4.9 %custom-call.8 = f32[2,1,32,32]{2,3,1,0:T(8,128)S(1)} custom-call(f32[2,1,32,32]{3,2,1,0:T(8,128)S(1)} %fusion.247), custom_call_target="InvertDiagBlocksLowerTriangular" | custom-call | tf_op jit(solution)/shard_map/while/body/eval_jaxpr/jit(_solve_triangular)/vmap()/triangular_solve | solution.py:125
  114.6 4.9 %custom-call.8 = f32[2,1,32,32]{2,3,1,0:T(8,128)S(1)} custom-call(f32[2,1,32,32]{3,2,1,0:T(8,128)S(1)} %fusion.247), custom_call_target="InvertDiagBlocksLowerTriangular" | custom-call | tf_op jit(solution)/shard_map/while/body/eval_jaxpr/jit(_solve_triangular)/vmap()/triangular_solve | solution.py:125
  126.6 4.9 %custom-call.8 = f32[2,1,32,32]{2,3,1,0:T(8,128)S(1)} custom-call(f32[2,1,32,32]{3,2,1,0:T(8,128)S(1)} %fusion.247), custom_call_target="InvertDiagBlocksLowerTriangular" | custom-call | tf_op jit(solution)/shard_map/while/body/eval_jaxpr/jit(_solve_triangular)/vmap()/triangular_solve | solution.py:125
  138.6 4.9 %custom-call.8 = f32[2,1,32,32]{2,3,1,0:T(8,128)S(1)} custom-call(f32[2,1,32,32]{3,2,1,0:T(8,128)S(1)} %fusion.247), custom_call_target="InvertDiagBlocksLowerTriangular" | custom-call | tf_op jit(solution)/shard_map/while/body/eval_jaxpr/jit(_solve_triangular)/vmap()/triangular_solve | solution.py:125
  147.6 7.8 %all-to-all-start.1 = ((bf16[16,256,64]{1,2,0:T(8,128)(2,1)}), bf16[16,256,64]{1,2,0:T(8,128)(2,1)S(1)}, u32[]{:S(2)}, u32[]{:S(2)}) async-start(bf16[16,256,64]{1,2,0:T(8,128)(2,1)} %broadcast_in_dim.107), calls=%async_computation.1 | async-start | bytes 1048576 | tf_op jit(solution)/shard_map/all_to_all | solution.py:12
  158.9 5.9 %all-gather.6.cloned.1.call-done = bf16[32,128,1,128]{3,1,2,0:T(8,128)(2,1)} async-done(((bf16[2,128,1,128]{3,1,2,0:T(8,128)(2,1)}), bf16[32,128,1,128]{3,1,2,0:T(8,128)(2,1)}) %all-gather.6.cloned.1.call-update) | async-done | bytes 1048592 | tf_op jit(solution)/shard_map/all_gather | solution.py:293
  164.8 45.0 %while.31 = (s32[]{:T(128)}, f32[128,1,128]{0,2,1:T(8,128)S(1)}, f32[1,128]{1,0:T(1,128)S(1)}, f32[1,128]{1,0:T(1,128)S(1)}, s32[]{:T(128)}, /*index=5*/bf16[16,...) while((s32[]{:T(128)}, f32[128,1,128]{0,2,1:T(8,128)S(1)}, ...), condition=%wide.region_18.19_spmd.clone, body=%wide.region_12.18_spmd.clone.sunk | while | flops 11075848 | bytes 960331 | solution.py:302
  167.7 3.0 %conditional.3 = ((f32[128,1,128]{0,2,1:T(8,128)S(1)}, f32[1,128]{1,0:T(1,128)S(1)}, f32[1,128]{1,0:T(1,128)S(1)})) conditional(s32[]{:T(128)} %convert_element_type.212, (f32[128,1,128]{0,2,1:T(8,128)S(1)}, f32[1,128]{1,0:T(1,128)S(1)}, f32[1,128]{1,0:T(1,128)S(1)}) %tuple.100, (s32[]{:T(128)}, bf16[16,2,128,1,128]{4,2,3,1,0:T(8,128)(2,1)}, ...), branch_computations={%region_13.13_spmd, %region_14.17_spmd} | conditional | flops 11075843 | bytes 959580 | solution.py:298
  170.7 3.0 %conditional.3 = ((f32[128,1,128]{0,2,1:T(8,128)S(1)}, f32[1,128]{1,0:T(1,128)S(1)}, f32[1,128]{1,0:T(1,128)S(1)})) conditional(s32[]{:T(128)} %convert_element_type.212, (f32[128,1,128]{0,2,1:T(8,128)S(1)}, f32[1,128]{1,0:T(1,128)S(1)}, f32[1,128]{1,0:T(1,128)S(1)}) %tuple.100, (s32[]{:T(128)}, bf16[16,2,128,1,128]{4,2,3,1,0:T(8,128)(2,1)}, ...), branch_computations={%region_13.13_spmd, %region_14.17_spmd} | conditional | flops 11075843 | bytes 959580 | solution.py:298
  173.7 3.0 %conditional.3 = ((f32[128,1,128]{0,2,1:T(8,128)S(1)}, f32[1,128]{1,0:T(1,128)S(1)}, f32[1,128]{1,0:T(1,128)S(1)})) conditional(s32[]{:T(128)} %convert_element_type.212, (f32[128,1,128]{0,2,1:T(8,128)S(1)}, f32[1,128]{1,0:T(1,128)S(1)}, f32[1,128]{1,0:T(1,128)S(1)}) %tuple.100, (s32[]{:T(128)}, bf16[16,2,128,1,128]{4,2,3,1,0:T(8,128)(2,1)}, ...), branch_computations={%region_13.13_spmd, %region_14.17_spmd} | conditional | flops 11075843 | bytes 959580 | solution.py:298
  176.7 3.0 %conditional.3 = ((f32[128,1,128]{0,2,1:T(8,128)S(1)}, f32[1,128]{1,0:T(1,128)S(1)}, f32[1,128]{1,0:T(1,128)S(1)})) conditional(s32[]{:T(128)} %convert_element_type.212, (f32[128,1,128]{0,2,1:T(8,128)S(1)}, f32[1,128]{1,0:T(1,128)S(1)}, f32[1,128]{1,0:T(1,128)S(1)}) %tuple.100, (s32[]{:T(128)}, bf16[16,2,128,1,128]{4,2,3,1,0:T(8,128)(2,1)}, ...), branch_computations={%region_13.13_spmd, %region_14.17_spmd} | conditional | flops 11075843 | bytes 959580 | solution.py:298
  179.7 3.0 %conditional.3 = ((f32[128,1,128]{0,2,1:T(8,128)S(1)}, f32[1,128]{1,0:T(1,128)S(1)}, f32[1,128]{1,0:T(1,128)S(1)})) conditional(s32[]{:T(128)} %convert_element_type.212, (f32[128,1,128]{0,2,1:T(8,128)S(1)}, f32[1,128]{1,0:T(1,128)S(1)}, f32[1,128]{1,0:T(1,128)S(1)}) %tuple.100, (s32[]{:T(128)}, bf16[16,2,128,1,128]{4,2,3,1,0:T(8,128)(2,1)}, ...), branch_computations={%region_13.13_spmd, %region_14.17_spmd} | conditional | flops 11075843 | bytes 959580 | solution.py:298
  182.7 3.0 %conditional.3 = ((f32[128,1,128]{0,2,1:T(8,128)S(1)}, f32[1,128]{1,0:T(1,128)S(1)}, f32[1,128]{1,0:T(1,128)S(1)})) conditional(s32[]{:T(128)} %convert_element_type.212, (f32[128,1,128]{0,2,1:T(8,128)S(1)}, f32[1,128]{1,0:T(1,128)S(1)}, f32[1,128]{1,0:T(1,128)S(1)}) %tuple.100, (s32[]{:T(128)}, bf16[16,2,128,1,128]{4,2,3,1,0:T(8,128)(2,1)}, ...), branch_computations={%region_13.13_spmd, %region_14.17_spmd} | conditional | flops 11075843 | bytes 959580 | solution.py:298
  185.7 3.0 %conditional.3 = ((f32[128,1,128]{0,2,1:T(8,128)S(1)}, f32[1,128]{1,0:T(1,128)S(1)}, f32[1,128]{1,0:T(1,128)S(1)})) conditional(s32[]{:T(128)} %convert_element_type.212, (f32[128,1,128]{0,2,1:T(8,128)S(1)}, f32[1,128]{1,0:T(1,128)S(1)}, f32[1,128]{1,0:T(1,128)S(1)}) %tuple.100, (s32[]{:T(128)}, bf16[16,2,128,1,128]{4,2,3,1,0:T(8,128)(2,1)}, ...), branch_computations={%region_13.13_spmd, %region_14.17_spmd} | conditional | flops 11075843 | bytes 959580 | solution.py:298
  188.7 3.0 %conditional.3 = ((f32[128,1,128]{0,2,1:T(8,128)S(1)}, f32[1,128]{1,0:T(1,128)S(1)}, f32[1,128]{1,0:T(1,128)S(1)})) conditional(s32[]{:T(128)} %convert_element_type.212, (f32[128,1,128]{0,2,1:T(8,128)S(1)}, f32[1,128]{1,0:T(1,128)S(1)}, f32[1,128]{1,0:T(1,128)S(1)}) %tuple.100, (s32[]{:T(128)}, bf16[16,2,128,1,128]{4,2,3,1,0:T(8,128)(2,1)}, ...), branch_computations={%region_13.13_spmd, %region_14.17_spmd} | conditional | flops 11075843 | bytes 959580 | solution.py:298
  191.8 3.0 %conditional.3 = ((f32[128,1,128]{0,2,1:T(8,128)S(1)}, f32[1,128]{1,0:T(1,128)S(1)}, f32[1,128]{1,0:T(1,128)S(1)})) conditional(s32[]{:T(128)} %convert_element_type.212, (f32[128,1,128]{0,2,1:T(8,128)S(1)}, f32[1,128]{1,0:T(1,128)S(1)}, f32[1,128]{1,0:T(1,128)S(1)}) %tuple.100, (s32[]{:T(128)}, bf16[16,2,128,1,128]{4,2,3,1,0:T(8,128)(2,1)}, ...), branch_computations={%region_13.13_spmd, %region_14.17_spmd} | conditional | flops 11075843 | bytes 959580 | solution.py:298
  194.8 3.0 %conditional.3 = ((f32[128,1,128]{0,2,1:T(8,128)S(1)}, f32[1,128]{1,0:T(1,128)S(1)}, f32[1,128]{1,0:T(1,128)S(1)})) conditional(s32[]{:T(128)} %convert_element_type.212, (f32[128,1,128]{0,2,1:T(8,128)S(1)}, f32[1,128]{1,0:T(1,128)S(1)}, f32[1,128]{1,0:T(1,128)S(1)}) %tuple.100, (s32[]{:T(128)}, bf16[16,2,128,1,128]{4,2,3,1,0:T(8,128)(2,1)}, ...), branch_computations={%region_13.13_spmd, %region_14.17_spmd} | conditional | flops 11075843 | bytes 959580 | solution.py:298
  197.8 3.0 %conditional.3 = ((f32[128,1,128]{0,2,1:T(8,128)S(1)}, f32[1,128]{1,0:T(1,128)S(1)}, f32[1,128]{1,0:T(1,128)S(1)})) conditional(s32[]{:T(128)} %convert_element_type.212, (f32[128,1,128]{0,2,1:T(8,128)S(1)}, f32[1,128]{1,0:T(1,128)S(1)}, f32[1,128]{1,0:T(1,128)S(1)}) %tuple.100, (s32[]{:T(128)}, bf16[16,2,128,1,128]{4,2,3,1,0:T(8,128)(2,1)}, ...), branch_computations={%region_13.13_spmd, %region_14.17_spmd} | conditional | flops 11075843 | bytes 959580 | solution.py:298
  216.5 10.2 %all-to-all-start.2 = ((bf16[8,16,2048]{2,1,0:T(8,128)(2,1)}), bf16[8,16,2048]{2,1,0:T(8,128)(2,1)S(1)}, u32[]{:S(2)}, u32[]{:S(2)}) async-start(bf16[8,16,2048]{2,1,0:T(8,128)(2,1)} %bitcast.66), calls=%async_computation.2 | async-start | bytes 1048576 | tf_op jit(solution)/shard_map/all_to_all | solution.py:88
  227.2 9.8 %all-to-all-done.2 = bf16[8,16,2048]{2,1,0:T(8,128)(2,1)S(1)} async-done(((bf16[8,16,2048]{2,1,0:T(8,128)(2,1)}), bf16[8,16,2048]{2,1,0:T(8,128)(2,1)S(1)}, u32[]{:S(2)}, u32[]{:S(2)}) %all-to-all-start.2) | async-done | bytes 524320 | tf_op jit(solution)/shard_map/all_to_all | solution.py:88
  (389 shorter events, 116.5 us)
Async XLA Ops:
  7.2 205.2 %copy-start = (bf16[128,2048]{1,0:T(8,128)(2,1)S(1)}, bf16[128,2048]{1,0:T(8,128)(2,1)}, u32[]{:S(2)}) copy-start(bf16[128,2048]{1,0:T(8,128)(2,1)} %param.48) | copy-start | bytes 1572868
  7.2 24.9 %copy-start.3 = (bf16[2048,64]{0,1:T(8,128)(2,1)S(1)}, bf16[2048,64]{0,1:T(8,128)(2,1)}, u32[]{:S(2)}) copy-start(bf16[2048,64]{0,1:T(8,128)(2,1)} %param.34) | copy-start | bytes 786436
  7.2 24.9 %copy-start.5 = (bf16[64,128]{1,0:T(8,128)(2,1)S(1)}, bf16[64,128]{1,0:T(8,128)(2,1)}, u32[]{:S(2)}) copy-start(bf16[64,128]{1,0:T(8,128)(2,1)} %param.35) | copy-start | bytes 49156
  7.2 24.9 %copy-start.7 = (f32[128]{0:T(128)S(1)}, f32[128]{0:T(128)}, u32[]{:S(2)}) copy-start(f32[128]{0:T(128)} %param.38) | copy-start | bytes 1540
  7.2 25.5 %copy-start.4 = (bf16[2048,64]{0,1:T(8,128)(2,1)S(1)}, bf16[2048,64]{0,1:T(8,128)(2,1)}, u32[]{:S(2)}) copy-start(bf16[2048,64]{0,1:T(8,128)(2,1)} %param.36) | copy-start | bytes 786436
  7.2 25.5 %copy-start.6 = (bf16[64,128]{1,0:T(8,128)(2,1)S(1)}, bf16[64,128]{1,0:T(8,128)(2,1)}, u32[]{:S(2)}) copy-start(bf16[64,128]{1,0:T(8,128)(2,1)} %param.37) | copy-start | bytes 49156
  7.2 25.5 %copy-start.8 = (f32[128]{0:T(128)S(1)}, f32[128]{0:T(128)}, u32[]{:S(2)}) copy-start(f32[128]{0:T(128)} %param.39) | copy-start | bytes 1540
  7.2 82.6 %all-gather.4.cloned.1.call-start = ((), (), s32[]{:S(2)}) async-start(), calls=%async_computation.3 | async-start | bytes 4456448 | tf_op jit(solution)/shard_map/all_gather | solution.py:34
  13.5 0.7 copy-start.2
  16.1 14.6 %all-to-all-start = ((bf16[8,128,256]{1,2,0:T(8,128)(2,1)}), bf16[8,128,256]{1,2,0:T(8,128)(2,1)S(1)}, u32[]{:S(2)}, u32[]{:S(2)}) async-start(bf16[8,128,256]{1,2,0:T(8,128)(2,1)} %broadcast_in_dim.74), calls=%async_computation | async-start | bytes 1048576 | tf_op jit(solution)/shard_map/all_to_all | solution.py:12
  20.4 144.4 %all-gather.6.cloned.1.call-start = ((), (), s32[]{:S(2)}) async-start(), calls=%async_computation.4 | async-start | bytes 1114112 | tf_op jit(solution)/shard_map/all_gather | solution.py:293
  147.6 62.3 %all-to-all-start.1 = ((bf16[16,256,64]{1,2,0:T(8,128)(2,1)}), bf16[16,256,64]{1,2,0:T(8,128)(2,1)S(1)}, u32[]{:S(2)}, u32[]{:S(2)}) async-start(bf16[16,256,64]{1,2,0:T(8,128)(2,1)} %broadcast_in_dim.107), calls=%async_computation.1 | async-start | bytes 1048576 | tf_op jit(solution)/shard_map/all_to_all | solution.py:12
  210.3 2.1 copy-start.9
  210.7 3.3 %copy-start.1 = (bf16[128,2048]{1,0:T(8,128)(2,1)S(1)}, bf16[128,2048]{1,0:T(8,128)(2,1)}, u32[]{:S(2)}) copy-start(bf16[128,2048]{1,0:T(8,128)(2,1)} %param.49) | copy-start | bytes 1572868
  216.5 20.6 %all-to-all-start.2 = ((bf16[8,16,2048]{2,1,0:T(8,128)(2,1)}), bf16[8,16,2048]{2,1,0:T(8,128)(2,1)S(1)}, u32[]{:S(2)}, u32[]{:S(2)}) async-start(bf16[8,16,2048]{2,1,0:T(8,128)(2,1)} %bitcast.66), calls=%async_computation.2 | async-start | bytes 1048576 | tf_op jit(solution)/shard_map/all_to_all | solution.py:88
Sparse Core Ops, SparseCore 0:
  14.4 75.4 all-gather.3
  93.4 71.2 all-gather.5
where the time goes:
time: 248 us; the launch traced here: 245 us
  waiting for transfers between devices  80.9 us (33%)
  matrix products  70.7 us (29%)
  other arithmetic  37.6 us (15%)
  starting transfers between devices  22.4 us (9%)
  local copies, waits for them, and re-layouts  16 us (6%)
  between operations  15.2 us (6%)
    all_gather x1, waiting for transfers between devices, in_one_piece(): lax.all_gather(both, axis, axis=dim, tiled=True)  56.6 us
    dot_general x16, matrix products, attend(): jnp.einsum('qhd,khd->hqk', query_heads, paired_piece[0], preferred_elemen...  24.5 us
    another operation x20, other arithmetic, block_pass(): jax.scipy.linalg.solve_triangular(weigh_steer + diagonal, entering, lower...  20.1 us
    dot_general x16, matrix products, attend(): jnp.einsum('hqk,khd->qhd', weights.astype(jnp.bfloat16), paired_piece[1],...  14.4 us
    all_to_all x2, starting transfers between devices, copy_for_each(): lax.all_to_all(jnp.broadcast_to(value[None], (devices, *value.shape)), ax...  12.1 us
    all_to_all x1, starting transfers between devices, sent_and_summed(): lax.all_to_all(cut_along(value, dim, devices), axis, 0, 0, tiled=True)  10.2 us
    all_to_all x1, waiting for transfers between devices, sent_and_summed(): lax.all_to_all(cut_along(value, dim, devices), axis, 0, 0, tiled=True)  9.8 us
    all_to_all x2, waiting for transfers between devices, copy_for_each(): lax.all_to_all(jnp.broadcast_to(value[None], (devices, *value.shape)), ax...  8.57 us
  transfers between devices with their start and end apart: 5, of which 4 were waited for; matrix products, arithmetic and copies ran while one was open for 44% of the time, Pallas kernels for 0%

commit v1 on v0

--- a/solution.py
+++ b/solution.py
@@ -290,7 +290,9 @@
         jnp.zeros((heads_b, row_count), jnp.float32),
     )
     running = attend(empty_b, paired, own_index)
-    all_pairs = lax.all_gather(paired[None], "sp", axis=0, tiled=True)
+    all_pairs = jnp.concatenate(
+        lax.all_to_all(jnp.stack([paired[None]] * lax.axis_size("sp")), "sp", 0, 0), axis=0
+    )
 
     def visit_piece(rounds, holding):
         source = own_index - rounds

time: 248 us -> 297 us (1.20)
  waiting for transfers between devices: 80.9 us -> 127 us
    all_to_all x0 -> x1, waiting for transfers between devices: none -> 37 us  [local(): lax.all_to_all(jnp.stack([paired[None]] * lax.axis_size('sp')), 'sp', 0, 0)]
    all_to_all x2, waiting for transfers between devices: 8.57 us -> 23.4 us  [copy_for_each(): lax.all_to_all(jnp.broadcast_to(value[None], (devices, *value.shape)), ax...]
    all_to_all x0 -> x1, starting transfers between devices: none -> 6.04 us  [local(): lax.all_to_all(jnp.stack([paired[None]] * lax.axis_size('sp')), 'sp', 0, 0)]
    all_gather x1 -> x0, waiting for transfers between devices: 5.9 us -> none  [local(): all_pairs = lax.all_gather(paired[None], 'sp', axis=0, tiled=True)]
    all_to_all x1, starting transfers between devices: 10.2 us -> 5.83 us  [sent_and_summed(): lax.all_to_all(cut_along(value, dim, devices), axis, 0, 0, tiled=True)]
  transfers between devices with their start and end apart: 5 -> 5, of which waited for: 4 -> 5; matrix products, arithmetic and copies ran while one was open for 44% -> 5% of each run, Pallas kernels for 0% -> 0%
where the time goes in v1:
time: 297 us; the launch traced here: 293 us
  waiting for transfers between devices  127 us (43%)
  matrix products  70.8 us (24%)
  other arithmetic  36.9 us (12%)
  starting transfers between devices  24 us (8%)
  local copies, waits for them, and re-layouts  17.3 us (6%)
  between operations  15.2 us (5%)
    all_gather x1, waiting for transfers between devices, in_one_piece(): lax.all_gather(both, axis, axis=dim, tiled=True)  56.6 us
    all_to_all x1, waiting for transfers between devices, local(): lax.all_to_all(jnp.stack([paired[None]] * lax.axis_size('sp')), 'sp', 0, 0)  37 us
    dot_general x16, matrix products, attend(): jnp.einsum('qhd,khd->hqk', query_heads, paired_piece[0], preferred_elemen...  24.5 us
    all_to_all x2, waiting for transfers between devices, copy_for_each(): lax.all_to_all(jnp.broadcast_to(value[None], (devices, *value.shape)), ax...  23.4 us
    another operation x20, other arithmetic, block_pass(): jax.scipy.linalg.solve_triangular(weigh_steer + diagonal, entering, lower...  20.1 us
    dot_general x16, matrix products, attend(): jnp.einsum('hqk,khd->qhd', weights.astype(jnp.bfloat16), paired_piece[1],...  14.4 us
    all_to_all x2, starting transfers between devices, copy_for_each(): lax.all_to_all(jnp.broadcast_to(value[None], (devices, *value.shape)), ax...  12.1 us
    all_to_all x1, waiting for transfers between devices, sent_and_summed(): lax.all_to_all(cut_along(value, dim, devices), axis, 0, 0, tiled=True)  9.8 us
  transfers between devices with their start and end apart: 5, of which 5 were waited for; matrix products, arithmetic and copies ran while one was open for 5% of the time, Pallas kernels for 0%

profile of v1, /device:TPU:504, one launch (start us, length us, event | category | flops | bytes accessed | tf_op | source)
XLA Modules:
  0.0 292.7 jit_solution(6616710769927708243)
XLA Ops:
  16.1 4.3 %all-to-all-start = ((bf16[8,128,256]{1,2,0:T(8,128)(2,1)}), bf16[8,128,256]{1,2,0:T(8,128)(2,1)S(1)}, u32[]{:S(2)}, u32[]{:S(2)}) async-start(bf16[8,128,256]{1,2,0:T(8,128)(2,1)} %broadcast_in_dim.72), calls=%async_computation | async-start | bytes 1048576 | tf_op jit(solution)/shard_map/all_to_all | solution.py:12
  22.1 8.6 %all-to-all-done = bf16[8,128,256]{1,2,0:T(8,128)(2,1)S(1)} async-done(((bf16[8,128,256]{1,2,0:T(8,128)(2,1)}), bf16[8,128,256]{1,2,0:T(8,128)(2,1)S(1)}, u32[]{:S(2)}, u32[]{:S(2)}) %all-to-all-start) | async-done | bytes 524320 | tf_op jit(solution)/shard_map/all_to_all | solution.py:12
  33.3 56.6 %all-gather.2.cloned.1.call-done = bf16[2048,1024]{1,0:T(8,128)(2,1)} async-done(((bf16[128,1024]{1,0:T(8,128)(2,1)}), bf16[2048,1024]{1,0:T(8,128)(2,1)}) %all-gather.2.cloned.1.call-update) | async-done | bytes 4194320 | tf_op jit(solution)/shard_map/all_gather | solution.py:34
  94.8 48.1 %while.30 = (s32[]{:T(128)}, f32[2,128,64]{1,2,0:T(8,128)S(1)}, f32[4,32,2,128]{3,1,0,2:T(8,128)S(1)}, f32[4,32,2,64]{3,2,1,0:T(2,128)S(1)}, bf16[4,32,2,64]{3,2...) while((s32[]{:T(128)}, f32[2,128,64]{1,2,0:T(8,128)S(1)}, ...), condition=%wide.region_6.7_spmd, body=%wide.region_2.6_spmd.sunk | while | flops 11161506 | bytes 3108997 | solution.py:235
  99.1 4.9 %custom-call.8 = f32[2,1,32,32]{2,3,1,0:T(8,128)S(1)} custom-call(f32[2,1,32,32]{3,2,1,0:T(8,128)S(1)} %fusion.247), custom_call_target="InvertDiagBlocksLowerTriangular" | custom-call | tf_op jit(solution)/shard_map/while/body/eval_jaxpr/jit(_solve_triangular)/vmap()/triangular_solve | solution.py:125
  111.2 4.9 %custom-call.8 = f32[2,1,32,32]{2,3,1,0:T(8,128)S(1)} custom-call(f32[2,1,32,32]{3,2,1,0:T(8,128)S(1)} %fusion.247), custom_call_target="InvertDiagBlocksLowerTriangular" | custom-call | tf_op jit(solution)/shard_map/while/body/eval_jaxpr/jit(_solve_triangular)/vmap()/triangular_solve | solution.py:125
  123.2 4.9 %custom-call.8 = f32[2,1,32,32]{2,3,1,0:T(8,128)S(1)} custom-call(f32[2,1,32,32]{3,2,1,0:T(8,128)S(1)} %fusion.247), custom_call_target="InvertDiagBlocksLowerTriangular" | custom-call | tf_op jit(solution)/shard_map/while/body/eval_jaxpr/jit(_solve_triangular)/vmap()/triangular_solve | solution.py:125
  135.2 4.9 %custom-call.8 = f32[2,1,32,32]{2,3,1,0:T(8,128)S(1)} custom-call(f32[2,1,32,32]{3,2,1,0:T(8,128)S(1)} %fusion.247), custom_call_target="InvertDiagBlocksLowerTriangular" | custom-call | tf_op jit(solution)/shard_map/while/body/eval_jaxpr/jit(_solve_triangular)/vmap()/triangular_solve | solution.py:125
  144.1 7.8 %all-to-all-start.1 = ((bf16[16,256,64]{1,2,0:T(8,128)(2,1)}), bf16[16,256,64]{1,2,0:T(8,128)(2,1)S(1)}, u32[]{:S(2)}, u32[]{:S(2)}) async-start(bf16[16,256,64]{1,2,0:T(8,128)(2,1)} %broadcast_in_dim.104), calls=%async_computation.1 | async-start | bytes 1048576 | tf_op jit(solution)/shard_map/all_to_all | solution.py:12
  156.8 14.8 %all-to-all-done.1 = bf16[16,256,64]{1,2,0:T(8,128)(2,1)S(1)} async-done(((bf16[16,256,64]{1,2,0:T(8,128)(2,1)}), bf16[16,256,64]{1,2,0:T(8,128)(2,1)S(1)}, u32[]{:S(2)}, u32[]{:S(2)}) %all-to-all-start.1) | async-done | bytes 524320 | tf_op jit(solution)/shard_map/all_to_all | solution.py:12
  172.8 6.0 %all-to-all-start.2 = ((bf16[16,1,2,128,1,128]{5,3,2,4,1,0:T(8,128)(2,1)}), bf16[16,1,2,128,1,128]{5,3,2,4,1,0:T(8,128)(2,1)}, u32[]{:S(2)}, u32[]{:S(2)}) async-start(bf16[16,1,2,128,1,128]{5,3,2,4,1,0:T(8,128)(2,1)} %stack.10), calls=%async_computation.2 | async-start | bytes 2097152 | tf_op jit(solution)/shard_map/all_to_all | solution.py:294
  184.5 37.0 %all-to-all-done.2 = bf16[16,1,2,128,1,128]{5,3,2,4,1,0:T(8,128)(2,1)} async-done(((bf16[16,1,2,128,1,128]{5,3,2,4,1,0:T(8,128)(2,1)}), bf16[16,1,2,128,1,128]{5,3,2,4,1,0:T(8,128)(2,1)}, u32[]{:S(2)}, u32[]{:S(2)}) %all-to-all-start.2) | async-done | bytes 1048608 | tf_op jit(solution)/shard_map/all_to_all | solution.py:294
  221.5 45.0 %while.31 = (s32[]{:T(128)}, f32[128,1,128]{0,2,1:T(8,128)S(1)}, f32[1,128]{1,0:T(1,128)S(1)}, f32[1,128]{1,0:T(1,128)S(1)}, s32[]{:T(128)}, /*index=5*/bf16[16,...) while((s32[]{:T(128)}, f32[128,1,128]{0,2,1:T(8,128)S(1)}, ...), condition=%wide.region_18.19_spmd.clone, body=%wide.region_12.18_spmd.clone.sunk | while | flops 11075848 | bytes 960331 | solution.py:304
  224.4 3.0 %conditional.3 = ((f32[128,1,128]{0,2,1:T(8,128)S(1)}, f32[1,128]{1,0:T(1,128)S(1)}, f32[1,128]{1,0:T(1,128)S(1)})) conditional(s32[]{:T(128)} %convert_element_type.212, (f32[128,1,128]{0,2,1:T(8,128)S(1)}, f32[1,128]{1,0:T(1,128)S(1)}, f32[1,128]{1,0:T(1,128)S(1)}) %tuple.100, (s32[]{:T(128)}, bf16[16,2,128,1,128]{4,2,3,1,0:T(8,128)(2,1)}, ...), branch_computations={%region_13.13_spmd, %region_14.17_spmd} | conditional | flops 11075843 | bytes 959580 | solution.py:300
  227.4 3.0 %conditional.3 = ((f32[128,1,128]{0,2,1:T(8,128)S(1)}, f32[1,128]{1,0:T(1,128)S(1)}, f32[1,128]{1,0:T(1,128)S(1)})) conditional(s32[]{:T(128)} %convert_element_type.212, (f32[128,1,128]{0,2,1:T(8,128)S(1)}, f32[1,128]{1,0:T(1,128)S(1)}, f32[1,128]{1,0:T(1,128)S(1)}) %tuple.100, (s32[]{:T(128)}, bf16[16,2,128,1,128]{4,2,3,1,0:T(8,128)(2,1)}, ...), branch_computations={%region_13.13_spmd, %region_14.17_spmd} | conditional | flops 11075843 | bytes 959580 | solution.py:300
  230.5 3.0 %conditional.3 = ((f32[128,1,128]{0,2,1:T(8,128)S(1)}, f32[1,128]{1,0:T(1,128)S(1)}, f32[1,128]{1,0:T(1,128)S(1)})) conditional(s32[]{:T(128)} %convert_element_type.212, (f32[128,1,128]{0,2,1:T(8,128)S(1)}, f32[1,128]{1,0:T(1,128)S(1)}, f32[1,128]{1,0:T(1,128)S(1)}) %tuple.100, (s32[]{:T(128)}, bf16[16,2,128,1,128]{4,2,3,1,0:T(8,128)(2,1)}, ...), branch_computations={%region_13.13_spmd, %region_14.17_spmd} | conditional | flops 11075843 | bytes 959580 | solution.py:300
  233.5 3.0 %conditional.3 = ((f32[128,1,128]{0,2,1:T(8,128)S(1)}, f32[1,128]{1,0:T(1,128)S(1)}, f32[1,128]{1,0:T(1,128)S(1)})) conditional(s32[]{:T(128)} %convert_element_type.212, (f32[128,1,128]{0,2,1:T(8,128)S(1)}, f32[1,128]{1,0:T(1,128)S(1)}, f32[1,128]{1,0:T(1,128)S(1)}) %tuple.100, (s32[]{:T(128)}, bf16[16,2,128,1,128]{4,2,3,1,0:T(8,128)(2,1)}, ...), branch_computations={%region_13.13_spmd, %region_14.17_spmd} | conditional | flops 11075843 | bytes 959580 | solution.py:300
  236.5 3.0 %conditional.3 = ((f32[128,1,128]{0,2,1:T(8,128)S(1)}, f32[1,128]{1,0:T(1,128)S(1)}, f32[1,128]{1,0:T(1,128)S(1)})) conditional(s32[]{:T(128)} %convert_element_type.212, (f32[128,1,128]{0,2,1:T(8,128)S(1)}, f32[1,128]{1,0:T(1,128)S(1)}, f32[1,128]{1,0:T(1,128)S(1)}) %tuple.100, (s32[]{:T(128)}, bf16[16,2,128,1,128]{4,2,3,1,0:T(8,128)(2,1)}, ...), branch_computations={%region_13.13_spmd, %region_14.17_spmd} | conditional | flops 11075843 | bytes 959580 | solution.py:300
  239.5 3.0 %conditional.3 = ((f32[128,1,128]{0,2,1:T(8,128)S(1)}, f32[1,128]{1,0:T(1,128)S(1)}, f32[1,128]{1,0:T(1,128)S(1)})) conditional(s32[]{:T(128)} %convert_element_type.212, (f32[128,1,128]{0,2,1:T(8,128)S(1)}, f32[1,128]{1,0:T(1,128)S(1)}, f32[1,128]{1,0:T(1,128)S(1)}) %tuple.100, (s32[]{:T(128)}, bf16[16,2,128,1,128]{4,2,3,1,0:T(8,128)(2,1)}, ...), branch_computations={%region_13.13_spmd, %region_14.17_spmd} | conditional | flops 11075843 | bytes 959580 | solution.py:300
  242.5 3.0 %conditional.3 = ((f32[128,1,128]{0,2,1:T(8,128)S(1)}, f32[1,128]{1,0:T(1,128)S(1)}, f32[1,128]{1,0:T(1,128)S(1)})) conditional(s32[]{:T(128)} %convert_element_type.212, (f32[128,1,128]{0,2,1:T(8,128)S(1)}, f32[1,128]{1,0:T(1,128)S(1)}, f32[1,128]{1,0:T(1,128)S(1)}) %tuple.100, (s32[]{:T(128)}, bf16[16,2,128,1,128]{4,2,3,1,0:T(8,128)(2,1)}, ...), branch_computations={%region_13.13_spmd, %region_14.17_spmd} | conditional | flops 11075843 | bytes 959580 | solution.py:300
  245.5 3.0 %conditional.3 = ((f32[128,1,128]{0,2,1:T(8,128)S(1)}, f32[1,128]{1,0:T(1,128)S(1)}, f32[1,128]{1,0:T(1,128)S(1)})) conditional(s32[]{:T(128)} %convert_element_type.212, (f32[128,1,128]{0,2,1:T(8,128)S(1)}, f32[1,128]{1,0:T(1,128)S(1)}, f32[1,128]{1,0:T(1,128)S(1)}) %tuple.100, (s32[]{:T(128)}, bf16[16,2,128,1,128]{4,2,3,1,0:T(8,128)(2,1)}, ...), branch_computations={%region_13.13_spmd, %region_14.17_spmd} | conditional | flops 11075843 | bytes 959580 | solution.py:300
  248.5 3.0 %conditional.3 = ((f32[128,1,128]{0,2,1:T(8,128)S(1)}, f32[1,128]{1,0:T(1,128)S(1)}, f32[1,128]{1,0:T(1,128)S(1)})) conditional(s32[]{:T(128)} %convert_element_type.212, (f32[128,1,128]{0,2,1:T(8,128)S(1)}, f32[1,128]{1,0:T(1,128)S(1)}, f32[1,128]{1,0:T(1,128)S(1)}) %tuple.100, (s32[]{:T(128)}, bf16[16,2,128,1,128]{4,2,3,1,0:T(8,128)(2,1)}, ...), branch_computations={%region_13.13_spmd, %region_14.17_spmd} | conditional | flops 11075843 | bytes 959580 | solution.py:300
  269.0 5.8 %all-to-all-start.3 = ((bf16[8,16,2048]{2,1,0:T(8,128)(2,1)}), bf16[8,16,2048]{2,1,0:T(8,128)(2,1)S(1)}, u32[]{:S(2)}, u32[]{:S(2)}) async-start(bf16[8,16,2048]{2,1,0:T(8,128)(2,1)} %bitcast.67), calls=%async_computation.3 | async-start | bytes 1048576 | tf_op jit(solution)/shard_map/all_to_all | solution.py:88
  275.4 9.8 %all-to-all-done.3 = bf16[8,16,2048]{2,1,0:T(8,128)(2,1)S(1)} async-done(((bf16[8,16,2048]{2,1,0:T(8,128)(2,1)}), bf16[8,16,2048]{2,1,0:T(8,128)(2,1)S(1)}, u32[]{:S(2)}, u32[]{:S(2)}) %all-to-all-start.3) | async-done | bytes 524320 | tf_op jit(solution)/shard_map/all_to_all | solution.py:88
  (389 shorter events, 123.0 us)
Async XLA Ops:
  7.2 175.6 %copy-start = (bf16[128,2048]{1,0:T(8,128)(2,1)S(1)}, bf16[128,2048]{1,0:T(8,128)(2,1)}, u32[]{:S(2)}) copy-start(bf16[128,2048]{1,0:T(8,128)(2,1)} %param.48) | copy-start | bytes 1572868
  7.2 24.9 %copy-start.3 = (bf16[2048,64]{0,1:T(8,128)(2,1)S(1)}, bf16[2048,64]{0,1:T(8,128)(2,1)}, u32[]{:S(2)}) copy-start(bf16[2048,64]{0,1:T(8,128)(2,1)} %param.34) | copy-start | bytes 786436
  7.2 24.9 %copy-start.5 = (bf16[64,128]{1,0:T(8,128)(2,1)S(1)}, bf16[64,128]{1,0:T(8,128)(2,1)}, u32[]{:S(2)}) copy-start(bf16[64,128]{1,0:T(8,128)(2,1)} %param.35) | copy-start | bytes 49156
  7.2 24.9 %copy-start.7 = (f32[128]{0:T(128)S(1)}, f32[128]{0:T(128)}, u32[]{:S(2)}) copy-start(f32[128]{0:T(128)} %param.38) | copy-start | bytes 1540
  7.2 25.5 %copy-start.4 = (bf16[2048,64]{0,1:T(8,128)(2,1)S(1)}, bf16[2048,64]{0,1:T(8,128)(2,1)}, u32[]{:S(2)}) copy-start(bf16[2048,64]{0,1:T(8,128)(2,1)} %param.36) | copy-start | bytes 786436
  7.2 25.5 %copy-start.6 = (bf16[64,128]{1,0:T(8,128)(2,1)S(1)}, bf16[64,128]{1,0:T(8,128)(2,1)}, u32[]{:S(2)}) copy-start(bf16[64,128]{1,0:T(8,128)(2,1)} %param.37) | copy-start | bytes 49156
  7.2 25.5 %copy-start.8 = (f32[128]{0:T(128)S(1)}, f32[128]{0:T(128)}, u32[]{:S(2)}) copy-start(f32[128]{0:T(128)} %param.39) | copy-start | bytes 1540
  7.2 82.6 %all-gather.2.cloned.1.call-start = ((), (), s32[]{:S(2)}) async-start(), calls=%async_computation.4 | async-start | bytes 4456448 | tf_op jit(solution)/shard_map/all_gather | solution.py:34
  13.5 0.7 copy-start.2
  16.1 14.6 %all-to-all-start = ((bf16[8,128,256]{1,2,0:T(8,128)(2,1)}), bf16[8,128,256]{1,2,0:T(8,128)(2,1)S(1)}, u32[]{:S(2)}, u32[]{:S(2)}) async-start(bf16[8,128,256]{1,2,0:T(8,128)(2,1)} %broadcast_in_dim.72), calls=%async_computation | async-start | bytes 1048576 | tf_op jit(solution)/shard_map/all_to_all | solution.py:12
  144.1 27.4 %all-to-all-start.1 = ((bf16[16,256,64]{1,2,0:T(8,128)(2,1)}), bf16[16,256,64]{1,2,0:T(8,128)(2,1)S(1)}, u32[]{:S(2)}, u32[]{:S(2)}) async-start(bf16[16,256,64]{1,2,0:T(8,128)(2,1)} %broadcast_in_dim.104), calls=%async_computation.1 | async-start | bytes 1048576 | tf_op jit(solution)/shard_map/all_to_all | solution.py:12
  172.8 48.7 %all-to-all-start.2 = ((bf16[16,1,2,128,1,128]{5,3,2,4,1,0:T(8,128)(2,1)}), bf16[16,1,2,128,1,128]{5,3,2,4,1,0:T(8,128)(2,1)}, u32[]{:S(2)}, u32[]{:S(2)}) async-start(bf16[16,1,2,128,1,128]{5,3,2,4,1,0:T(8,128)(2,1)} %stack.10), calls=%async_computation.2 | async-start | bytes 2097152 | tf_op jit(solution)/shard_map/all_to_all | solution.py:294
  180.7 2.1 copy-start.9
  182.8 83.8 %copy-start.1 = (bf16[128,2048]{1,0:T(8,128)(2,1)S(1)}, bf16[128,2048]{1,0:T(8,128)(2,1)}, u32[]{:S(2)}) copy-start(bf16[128,2048]{1,0:T(8,128)(2,1)} %param.49) | copy-start | bytes 1572868
  269.0 16.1 %all-to-all-start.3 = ((bf16[8,16,2048]{2,1,0:T(8,128)(2,1)}), bf16[8,16,2048]{2,1,0:T(8,128)(2,1)S(1)}, u32[]{:S(2)}, u32[]{:S(2)}) async-start(bf16[8,16,2048]{2,1,0:T(8,128)(2,1)} %bitcast.67), calls=%async_computation.3 | async-start | bytes 1048576 | tf_op jit(solution)/shard_map/all_to_all | solution.py:88
Sparse Core Ops, SparseCore 0:
  14.4 75.4 all-gather.1
